TPU v7x, 32 devices: a whole 2x2x4 slice. The times are simulated.
32 devices in a mesh: row: 16 (over z, y, x), col: 2 (over core).
Axes of the slice: x: 2, y: 2, z: 4, core: 2. Of those that a mesh axis runs over, the one named last changes fastest.
Arguments:
- tokens: bfloat16 [2, 6144, 2048], P('col', 'row'), may hold values from -6 to 6
- norm_gain: bfloat16 [2048], replicated, may hold values from 0.099609375 to 1.8984375
- in_weight: bfloat16 [2048, 512], P('row', 'col'), may hold values from -0.125 to 0.125
- out_weight: bfloat16 [512, 2048], P('col', 'row'), may hold values from -0.25 to 0.25
Outputs:
- mixed: bfloat16 [2, 6144, 2048], P('col', 'row')
All inputs are finite; a program needn't handle non-finite values.
Results may differ from a plain program's by a relative error of at most 0.013.
Values may be sent and summed in bfloat16 or wider, within the bound.
A program may use at most 64 MiB of HBM per device.

v0:
```python
import functools
import math

import jax
import jax.numpy as jnp
import numpy as np
from jax import lax
from jax.experimental import pallas as pl
from jax.experimental.pallas import tpu as pltpu
from jax.sharding import PartitionSpec as P

GS = 64
EPS = 1e-06
LANES = 128
F32 = jnp.float32
BF16 = jnp.bfloat16


def angles(left, right, modulus):
    product = np.arange(left)[:, None] * np.arange(right)[None, :] % modulus
    radians = product * (2.0 * math.pi / modulus)
    return np.cos(radians), np.sin(radians)


def channel_tables(narrow):
    cos, sin = angles(GS, GS, GS)
    half = narrow // 2
    forward = np.zeros((GS, GS))
    combine = np.zeros((GS, GS))
    for slot in range(GS):
        owner, place = divmod(slot, narrow)
        j = owner * half + place % half
        if place >= half and j > 0:
            forward[slot] = sin[j]
            combine[slot, j] = -1.0
            combine[slot, GS - j] = 1.0
        else:
            j = GS // 2 if place >= half else j
            forward[slot] = cos[j]
            combine[slot, j] = 1.0
            combine[slot, (GS - j) % GS] = 1.0
    copies = np.eye(LANES // GS)
    return np.kron(copies, forward), np.kron(copies, combine)


def tables(peers, rows, channels):
    narrow = channels // peers
    step = rows // peers
    length = peers * rows
    forward, combine = channel_tables(narrow)
    cos, sin = angles(peers, peers, peers)
    eye = np.eye(narrow)
    chunk = LANES // narrow
    first = np.concatenate(
        [
            np.kron(part[t : t + chunk], eye)
            for t in range(0, peers, chunk)
            for part in (cos, -sin)
        ]
    )
    turn = np.stack(angles(peers, rows, length)) / math.sqrt(length * GS)
    second = np.concatenate(angles(rows, rows, rows), axis=1)
    order = np.zeros((rows, rows))
    for t in range(peers):
        for u in range(step):
            order[u * peers + t, t * step + u] = 1.0
    return (
        jnp.asarray(forward, BF16),
        jnp.asarray(combine, BF16),
        jnp.asarray(first, BF16),
        jnp.asarray(turn, F32),
        jnp.asarray(second, BF16),
        jnp.asarray(order, BF16),
    )


def gather_orders(peers):
    short = []
    stride, rest = 1, peers
    while len(short) < 2 and rest % 2 == 0:
        short.append((stride, 2))
        stride, rest = stride * 2, rest // 2
    long = [(stride, rest)] if rest > 1 else []
    return [long + short, long + short[::-1]]


def dot(a, b):
    return jnp.dot(a, b, preferred_element_type=F32)


def dot_nt(a, b):
    return lax.dot_general(a, b, (((1,), (1,)), ((), ())), preferred_element_type=F32)


def kernel(
    peers,
    cols,
    tokens_hbm,
    gain_ref,
    in_ref,
    out_w_ref,
    forward_ref,
    combine_ref,
    first_hbm,
    turn_hbm,
    second_hbm,
    order_hbm,
    result_ref,
    result,
    tokens,
    first,
    turn,
    second,
    order,
    normed,
    projected,
    w_in,
    w_out,
    send_one,
    got_one,
    lines,
    send_two,
    got_two,
    arranged,
    local_sem,
    own_sem,
    store_sem,
    g_send,
    g_recv,
    c_send,
    c_recv,
    x_send,
    x_recv,
):
    me = lax.axis_index("row")
    core = lax.axis_index("col")
    rows, width = tokens.shape
    channels = first.shape[1]
    parts = g_send.shape[1]
    orders = gather_orders(peers)
    stages = len(orders[0])
    narrow = channels // peers
    half = narrow // 2
    step = rows // peers

    loads = [
        pltpu.make_async_copy(src, dst, local_sem.at[i])
        for i, (src, dst) in enumerate(
            (
                (tokens_hbm, tokens),
                (first_hbm, first),
                (turn_hbm, turn),
                (second_hbm, second),
                (order_hbm, order),
            )
        )
    ]
    for load in loads:
        load.start()

    def peer(o):
        return lax.rem(me + o, peers)

    def mate(o):
        return lax.rem(core + o, cols)

    barrier = pltpu.get_barrier_semaphore()
    for o in range(1, peers):
        pl.semaphore_signal(barrier, inc=1, device_id={"row": peer(o)})
    for o in range(1, cols):
        pl.semaphore_signal(barrier, inc=1, device_id={"col": mate(o)})
    pl.semaphore_wait(barrier, peers - 1 + cols - 1)

    class Gather:
        def __init__(self, which, src, buffer):
            self.which, self.src, self.buffer = which, src, buffer
            self.height = src.shape[0] // parts
            self.held = [[None] for _ in range(parts)]
            self.open = [[] for _ in range(parts)]
            self.sent = []
            self.count = [0] * parts
            self.own = pltpu.make_async_copy(src, buffer.at[core, me], own_sem.at[which])
            self.own.start()

        def issue(self, part, stage):
            stride, size = orders[part % len(orders)][stage]
            at = pl.ds(part * self.height, self.height)
            place = lax.rem(lax.div(me, stride), size)
            arrived = []
            for o in range(1, size):
                to = me + (lax.rem(place + o, size) - place) * stride
                origin = (lax.rem(place + size - o, size) - place) * stride
                for held in self.held[part]:
                    block = me if held is None else held
                    copy = pltpu.make_async_remote_copy(
                        src_ref=self.src.at[at]
                        if held is None
                        else self.buffer.at[core, block, at],
                        dst_ref=self.buffer.at[core, block, at],
                        send_sem=g_send.at[self.which, part, self.count[part]],
                        recv_sem=g_recv.at[self.which, part, self.count[part]],
                        device_id={"row": to},
                    )
                    copy.start()
                    self.count[part] += 1
                    self.open[part].append(copy)
                    self.sent.append(copy)
                    arrived.append(block + origin)
            self.held[part] += arrived

        def wait(self, part):
            for copy in self.open[part]:
                copy.wait_recv()
            self.open[part] = []

        def advance(self, stage):
            for part in range(parts):
                self.wait(part)
                self.issue(part, stage)

        def relay(self):
            self.own.wait()
            self.passed = []
            for part in range(parts):
                self.wait(part)
                at = pl.ds(part * self.height, self.height)
                for o in range(1, cols):
                    copy = pltpu.make_async_remote_copy(
                        src_ref=self.buffer.at[core, :, at],
                        dst_ref=self.buffer.at[core, :, at],
                        send_sem=c_send.at[self.which, part, o],
                        recv_sem=c_recv.at[self.which, part, o],
                        device_id={"col": mate(o)},
                    )
                    copy.start()
                    self.passed.append(copy)

        def finish(self):
            for copy in self.passed:
                copy.wait_recv()

    gather_in = Gather(0, in_ref, w_in)
    gather_out = Gather(1, out_w_ref, w_out)
    gather_in.advance(0)

    loads[0].wait()
    gain = gain_ref[...].astype(F32).reshape(1, width)
    tile = 32

    def norm(i, carry):
        at = pl.ds(pl.multiple_of(i * tile, tile), tile)
        block = tokens[at, :].astype(F32)
        inverse = lax.rsqrt(jnp.mean(block * block, axis=-1, keepdims=True) + EPS)
        normed[at, :] = (block * inverse * gain).astype(BF16)
        return carry

    tiles = rows // tile
    cuts = [tiles * i // stages for i in range(stages + 1)]
    for stage in range(stages):
        if stage:
            gather_in.advance(stage)
        lax.fori_loop(cuts[stage], cuts[stage + 1], norm, 0)
    gather_out.advance(0)
    gather_in.relay()

    part = channels // cols
    for i in range(cols):
        if i == 1:
            gather_in.finish()
        c = mate(i)
        projected[c] = dot(normed[...], w_in[c].reshape(width, part)).astype(BF16)

    natural_channels = jnp.concatenate([projected[c] for c in range(cols)], axis=1)
    for b in range(0, channels, LANES):
        slots = dot_nt(forward_ref[...], natural_channels[:, b : b + LANES]).astype(BF16)
        send_one[b // narrow : (b + LANES) // narrow] = slots.reshape(
            LANES // narrow, narrow, rows
        )

    def exchange(which, src, dst):
        copies = []
        for o in range(1, peers):
            copy = pltpu.make_async_remote_copy(
                src_ref=src.at[peer(o)],
                dst_ref=dst.at[me],
                send_sem=x_send.at[which, o],
                recv_sem=x_recv.at[which, o],
                device_id={"row": peer(o)},
            )
            copy.start()
            copies.append(copy)
        own = pltpu.make_async_copy(src.at[me], dst.at[me], x_send.at[which, 0])
        own.start()
        return copies, own

    def land(copies, own):
        for copy in copies:
            copy.wait_recv()
        own.wait()

    one_copies, one_own = exchange(0, send_one, got_one)
    if stages > 1:
        gather_out.advance(1)
    land(one_copies, one_own)
    for stage in range(2, stages):
        gather_out.advance(stage)
    for load in loads[1:]:
        load.wait()
    columns = got_one[...].reshape(channels, rows)
    place = lax.broadcasted_iota(jnp.int32, (narrow, rows), 0)
    leads = lax.rem(me * narrow, GS) == 0
    first_sine = jnp.where(leads, half + 1, half)
    sine = place >= first_sine
    chunk = LANES // narrow
    for t0 in range(0, peers, chunk):
        both = dot(first[2 * t0 * narrow : 2 * (t0 + chunk) * narrow, :], columns)
        for i in range(chunk):
            t = t0 + i
            real = both[i * narrow : (i + 1) * narrow]
            imag = both[LANES + i * narrow : LANES + (i + 1) * narrow]
            cos = turn[0, t : t + 1, :]
            sin = turn[1, t : t + 1, :]
            z_real = real * cos + imag * sin
            z_imag = imag * cos - real * sin
            at = slice(t * narrow, (t + 1) * narrow)
            lines[at, :rows] = jnp.where(sine, -z_imag, z_real)
            lines[at, rows:] = jnp.where(sine, z_real, z_imag)
    whole = dot_nt(second[...], lines[...].astype(BF16))
    send_two[...] = whole.reshape(peers, step, channels).astype(BF16)
    two_copies, two_own = exchange(1, send_two, got_two)
    gather_out.relay()
    land(two_copies, two_own)

    block_of = lax.broadcasted_iota(jnp.int32, (step, LANES), 1) // narrow
    for d0 in range(0, peers, chunk):
        for t0 in range(0, peers, chunk):
            held = [
                got_two[d0 + i, :, t0 * narrow : (t0 + chunk) * narrow].astype(F32)
                for i in range(chunk)
            ]
            for j in range(chunk):
                made = None
                for i in range(chunk):
                    shift = (i - j) * narrow % LANES
                    moved = pltpu.roll(held[i], shift, 1) if shift else held[i]
                    made = moved if made is None else jnp.where(block_of == i, moved, made)
                t = t0 + j
                arranged[t * step : (t + 1) * step, d0 * narrow : (d0 + chunk) * narrow] = made
    natural = dot(order[...], arranged[...].astype(BF16)).astype(BF16)
    mixed = jnp.concatenate(
        [
            dot(natural[:, b : b + LANES], combine_ref[...]).astype(BF16)
            for b in range(0, channels, LANES)
        ],
        axis=1,
    )
    gather_out.finish()
    stores = []
    wide = w_out.shape[3]
    group = max(1, 256 // wide)
    for p in range(0, peers, group):
        weight = jnp.concatenate(
            [w_out[:, p + i].reshape(channels, wide) for i in range(group)], axis=1
        )
        at = slice(p * wide, (p + group) * wide)
        result[:, at] = dot(mixed, weight).astype(BF16)
        store = pltpu.make_async_copy(result.at[:, at], result_ref.at[:, at], store_sem.at[p])
        store.start()
        stores.append(store)
    for store in stores:
        store.wait()

    for copy in (
        gather_in.sent
        + gather_in.passed
        + gather_out.sent
        + gather_out.passed
        + one_copies
        + two_copies
    ):
        copy.wait_send()


def body(peers, cols, tokens, norm_gain, in_weight, out_weight):
    rows, width = tokens.shape[1:]
    in_rows, in_cols = in_weight.shape
    out_rows, out_cols = out_weight.shape
    channels = in_cols * cols
    narrow = channels // peers
    step = rows // peers
    parts = max(1, min(4, in_rows // 16, out_rows // 16))
    forward, combine, first, turn, second, order = tables(peers, rows, channels)
    vmem = pl.BlockSpec(memory_space=pltpu.VMEM)
    hbm = pl.BlockSpec(memory_space=pl.ANY)
    result = pl.pallas_call(
        functools.partial(kernel, peers, cols),
        out_shape=jax.ShapeDtypeStruct((rows, width), BF16),
        in_specs=[hbm, vmem, vmem, vmem, vmem, vmem, hbm, hbm, hbm, hbm],
        out_specs=hbm,
        scratch_shapes=[
            pltpu.VMEM((rows, width), BF16),
            pltpu.VMEM((rows, width), BF16),
            pltpu.VMEM(first.shape, BF16),
            pltpu.VMEM(turn.shape, F32),
            pltpu.VMEM(second.shape, BF16),
            pltpu.VMEM(order.shape, BF16),
            pltpu.VMEM((rows, width), BF16),
            pltpu.VMEM((cols, rows, in_cols), BF16),
            pltpu.VMEM((cols, peers, in_rows, in_cols), BF16),
            pltpu.VMEM((cols, peers, out_rows, out_cols), BF16),
            pltpu.VMEM((peers, narrow, rows), BF16),
            pltpu.VMEM((peers, narrow, rows), BF16),
            pltpu.VMEM((channels, 2 * rows), F32),
            pltpu.VMEM((peers, step, channels), BF16),
            pltpu.VMEM((peers, step, channels), BF16),
            pltpu.VMEM((rows, channels), F32),
            pltpu.SemaphoreType.DMA((5,)),
            pltpu.SemaphoreType.DMA((2,)),
            pltpu.SemaphoreType.DMA((peers,)),
            pltpu.SemaphoreType.DMA((2, parts, peers)),
            pltpu.SemaphoreType.DMA((2, parts, peers)),
            pltpu.SemaphoreType.DMA((2, parts, cols)),
            pltpu.SemaphoreType.DMA((2, parts, cols)),
            pltpu.SemaphoreType.DMA((2, peers)),
            pltpu.SemaphoreType.DMA((2, peers)),
        ],
        compiler_params=pltpu.CompilerParams(
            collective_id=0, has_side_effects=True, vmem_limit_bytes=60 * 1024 * 1024
        ),
    )(tokens[0], norm_gain, in_weight, out_weight, forward, combine, first, turn, second, order)
    return result[None]


def solution(mesh):
    in_specs = (P("col", "row", None), P(), P("row", "col"), P("col", "row"))
    out_specs = P("col", "row", None)
    step = functools.partial(body, mesh.shape["row"], mesh.shape["col"])
    return jax.shard_map(step, mesh=mesh, in_specs=in_specs, out_specs=out_specs, check_vma=False)
```

profile of v0, /device:TPU:0, one launch (start us, length us, event | category | flops | bytes accessed | tf_op | source)
XLA Modules:
  0.0 55.4 jit_solution(17337185744508866284)
XLA Ops:
  0.0 52.6 %shard_map.100 = bf16[384,2048]{1,0:T(8,128)(2,1)} custom-call(bf16[384,2048]{1,0:T(8,128)(2,1)} %bitcast.3, bf16[2048]{0:T(1024)(128)(2,1)} %gain_ref.1, bf16[128,256]{1,0:T(8,128)(2,1)} %in_ref.1, bf16[256,128]{1,0:T(8,128)(2,1)} %out_w_ref.1, bf16[128,128]{1,0:T(8,128)(2,1)} %constant.12.clone.forward_ref, bf16[128,128]{1,0:T(8,128)(2,1)} %constant.13.clone.combine_ref, ...), custom_call_target="tpu_custom_call" | custom-call | tf_op jit(solution)/shard_map/pallas_call | solution.py:395
  52.7 2.7 %copy.12 = bf16[1,384,2048]{2,1,0:T(8,128)(2,1)} copy(bf16[1,384,2048]{2,1,0:T(8,128)(2,1)} %bitcast.2) | data formatting | bytes 3145728
where the time goes:
time: 55.6 us; the launch traced here: 55.4 us
  Pallas kernels  52.6 us (95%)
  local copies, waits for them, and re-layouts  2.73 us (5%)
    pallas_call x1, Pallas kernels, body(): pl.pallas_call(functools.partial(kernel, peers, cols), out_shape=jax.Shap...  52.6 us
    unnamed x1, local copies, waits for them, and re-layouts  2.73 us

commit v1 on v0

v1 whole, which is shorter than its diff:
```python
import functools
import math

import jax
import jax.numpy as jnp
import numpy as np
from jax import lax
from jax.experimental import pallas as pl
from jax.experimental.pallas import tpu as pltpu
from jax.sharding import PartitionSpec as P

GS = 64
EPS = 1e-06
LANES = 128
F32 = jnp.float32
BF16 = jnp.bfloat16


def angles(left, right, modulus):
    product = np.arange(left)[:, None] * np.arange(right)[None, :] % modulus
    radians = product * (2.0 * math.pi / modulus)
    return np.cos(radians), np.sin(radians)


def channel_tables(narrow):
    cos, sin = angles(GS, GS, GS)
    half = narrow // 2
    forward = np.zeros((GS, GS))
    place_of = np.zeros((GS, GS))
    for slot in range(GS):
        owner, place = divmod(slot, narrow)
        j = owner * half + place % half
        if place < half:
            forward[slot] = cos[j]
            place_of[slot, j] = 1.0
        elif j == 0:
            forward[slot] = cos[GS // 2]
            place_of[slot, GS // 2] = 1.0
        else:
            forward[slot] = sin[j]
            place_of[slot, GS - j] = 1.0
    copies = np.eye(LANES // GS)
    return np.kron(copies, forward), np.kron(copies, place_of)


def tables(peers, rows, narrow):
    length = peers * rows
    forward, place_of = channel_tables(narrow)
    cos, sin = angles(peers, peers, peers)
    eye = np.eye(narrow)
    chunk = LANES // narrow
    first = np.concatenate(
        [
            np.kron(part[t : t + chunk], eye)
            for t in range(0, peers, chunk)
            for part in (cos, -sin)
        ]
    )
    turn = np.stack(angles(peers, rows, length)) / math.sqrt(length * GS)
    second = np.concatenate(angles(rows, rows, rows), axis=1)
    return (
        jnp.asarray(forward, BF16),
        jnp.asarray(place_of, BF16),
        jnp.asarray(first, BF16),
        jnp.asarray(turn, F32),
        jnp.asarray(second, BF16),
    )


def grid_of(peers):
    a = 2 if peers % 2 == 0 else 1
    b = 2 if peers // a % 2 == 0 else 1
    return peers // (a * b), b, a


def dot(a, b):
    return jnp.dot(a, b, preferred_element_type=F32)


def dot_nt(a, b):
    return lax.dot_general(a, b, (((1,), (1,)), ((), ())), preferred_element_type=F32)


def far_first(depth):
    return sorted(range(depth), key=lambda o: abs(2 * o - depth))


class Sems:
    def __init__(self, send, recv):
        self.send, self.recv, self.used = send, recv, 0

    def next(self):
        i = self.used
        self.used += 1
        assert i < self.send.shape[0]
        return self.send.at[i], self.recv.at[i]


def sem_count(peers, cols, gathers):
    depth, b, a = grid_of(peers)
    each = depth - 1 + (a - 1) + (b - 1) + cols - 1
    return gathers * each + 4 * (peers - 1)


def kernel(
    peers,
    cols,
    chunks,
    in_parts,
    out_parts,
    tokens_hbm,
    gain_hbm,
    in_hbm,
    out_w_hbm,
    forward_hbm,
    place_hbm,
    first_hbm,
    turn_hbm,
    second_hbm,
    mixed_ref,
    weight_ref,
    tokens,
    gain,
    forward,
    place_of,
    first,
    turn,
    second,
    normed,
    w_in,
    w_out,
    send_one,
    got_one,
    lines,
    send_two,
    got_two,
    arranged,
    load_sem,
    own_sem,
    send_sem,
    recv_sem,
):
    me = lax.axis_index("row")
    core = lax.axis_index("col")
    rows, width = tokens.shape
    depth, tall, wide = grid_of(peers)
    x = lax.rem(me, wide)
    y = lax.rem(lax.div(me, wide), tall)
    z = lax.div(me, wide * tall)
    block = w_in.shape[-1]
    span = cols * block
    narrow = span // peers
    half = narrow // 2
    step = rows // peers
    group = LANES // narrow
    sems = Sems(send_sem, recv_sem)

    def at_peer(dz, dy, dx):
        tz = lax.rem(z + dz, depth)
        ty = lax.rem(y + dy, tall)
        tx = lax.rem(x + dx, wide)
        return (tz * tall + ty) * wide + tx

    def mate(o):
        return lax.rem(core + o, cols)

    near = [(o, 0, 0) for o in range(1, depth)]
    near += [(0, o, 0) for o in range(1, tall)] + [(0, 0, o) for o in range(1, wide)]

    barrier = pltpu.get_barrier_semaphore()
    for o in near:
        pl.semaphore_signal(barrier, inc=1, device_id={"row": at_peer(*o)})
    for o in range(1, cols):
        pl.semaphore_signal(barrier, inc=1, device_id={"col": mate(o)})

    owns = [
        pltpu.make_async_copy(
            in_hbm.at[:, c * block : (c + 1) * block], w_in.at[c, core, z, y, x], own_sem.at[c]
        )
        for c in range(chunks)
    ]
    owns.append(pltpu.make_async_copy(out_w_hbm, w_out.at[core, z, y, x], own_sem.at[chunks]))
    loads = [
        pltpu.make_async_copy(src, dst, load_sem.at[i])
        for i, (src, dst) in enumerate(
            (
                (tokens_hbm, tokens),
                (gain_hbm, gain),
                (forward_hbm, forward),
                (place_hbm, place_of),
                (first_hbm, first),
                (turn_hbm, turn),
                (second_hbm, second),
            )
        )
    ]
    for load in owns[:chunks] + loads[:2] + owns[chunks:] + loads[2:]:
        load.start()
    for own in owns[:chunks]:
        own.wait()
    pl.semaphore_wait(barrier, len(near) + cols - 1)

    sent = []

    def remote(src, dst, device):
        send, recv = sems.next()
        copy = pltpu.make_async_remote_copy(
            src_ref=src, dst_ref=dst, send_sem=send, recv_sem=recv, device_id=device
        )
        copy.start()
        sent.append(copy)
        return copy

    class Part:
        def __init__(self, buffer, index, height):
            self.buffer, self.at, self.flip = buffer, pl.ds(index * height, height), index % 2
            self.stage, self.open = 0, []

        def push(self):
            for copy in self.open:
                copy.wait_recv()
            held, everything = self.buffer.at[core], slice(None)
            if self.stage == 0:
                targets = [
                    (held.at[z, y, x, self.at], {"row": at_peer(o, 0, 0)})
                    for o in far_first(depth)
                    if o
                ]
            elif self.stage == 3:
                targets = [
                    (held.at[:, :, :, self.at], {"col": mate(o)}) for o in range(1, cols)
                ]
            else:
                along_x = (self.stage == 1) != bool(self.flip)
                if self.stage == 1:
                    ref = held.at[:, y, x, self.at]
                elif along_x:
                    ref = held.at[:, :, x, self.at]
                else:
                    ref = held.at[:, y, :, self.at]
                extent = wide if along_x else tall
                targets = [
                    (ref, {"row": at_peer(0, 0, o) if along_x else at_peer(0, o, 0)})
                    for o in range(1, extent)
                ]
            self.open = [remote(ref, ref, device) for ref, device in targets]
            self.stage += 1

        def finish(self):
            for copy in self.open:
                copy.wait_recv()

    def parts_of(buffer, count):
        height = buffer.shape[-2] // count
        return [Part(buffer, i, height) for i in range(count)]

    gather_in = [parts_of(w_in.at[c], in_parts) for c in range(chunks)]
    gather_out = parts_of(w_out, out_parts)
    def push(parts):
        for part in parts:
            part.push()

    push(gather_in[0])

    loads[0].wait()
    loads[1].wait()
    scale = gain[...].astype(F32).reshape(1, width)
    tile = 32

    def norm(i, carry):
        at = pl.ds(pl.multiple_of(i * tile, tile), tile)
        rows_of = tokens[at, :].astype(F32)
        inverse = lax.rsqrt(jnp.mean(rows_of * rows_of, axis=-1, keepdims=True) + EPS)
        normed[at, :] = (rows_of * inverse * scale).astype(BF16)
        return carry

    lax.fori_loop(0, rows // tile, norm, 0)

    push(gather_in[0])
    for c in range(1, chunks):
        push(gather_in[c])
    push(gather_in[0])
    for c in range(1, chunks):
        push(gather_in[c])
    owns[chunks].wait()
    push(gather_out)
    push(gather_in[0])
    for c in range(1, chunks):
        push(gather_in[c])
    for load in loads[2:]:
        load.wait()

    flights = {}

    def exchange(which, c, src, dst):
        copies = []
        for dz in far_first(depth):
            for dy in reversed(range(tall)):
                for dx in reversed(range(wide)):
                    if dz or dy or dx:
                        to = at_peer(dz, dy, dx)
                        copies.append(remote(src.at[to], dst.at[me], {"row": to}))
        own = pltpu.make_async_copy(src.at[me], dst.at[me], own_sem.at[chunks + 1])
        own.start()
        own.wait()
        flights[which, c] = copies

    def land(which, c):
        for copy in flights[which, c]:
            copy.wait_recv()

    def project(c):
        weight = jnp.concatenate(
            [w_in[c, i].reshape(width, block) for i in range(cols)], axis=1
        )
        projected = dot(normed[...], weight).astype(BF16)
        for b in range(0, span, LANES):
            slots = dot_nt(forward[...], projected[:, b : b + LANES]).astype(BF16)
            send_one[c, b // narrow : (b + LANES) // narrow] = slots.reshape(
                group, narrow, rows
            )

    leads = lax.rem(me * narrow, GS) == 0
    alone = (lax.broadcasted_iota(jnp.int32, (half, rows), 0) == 0) & leads

    def transform(c):
        columns = got_one[c].reshape(span, rows)
        for t0 in range(0, peers, group):
            both = dot(first[2 * t0 * narrow : 2 * (t0 + group) * narrow, :], columns)
            for i in range(group):
                t = t0 + i
                real = both[i * narrow : (i + 1) * narrow]
                imag = both[LANES + i * narrow : LANES + (i + 1) * narrow]
                cos = turn[0, t : t + 1, :]
                sin = turn[1, t : t + 1, :]
                z_real = real * cos + imag * sin
                z_imag = imag * cos - real * sin
                c_real, s_real = z_real[:half], z_real[half:]
                c_imag, s_imag = z_imag[:half], z_imag[half:]
                low = slice(t * narrow, t * narrow + half)
                high = slice(t * narrow + half, (t + 1) * narrow)
                lines[low, :rows] = jnp.where(alone, c_real, c_real + s_imag)
                lines[low, rows:] = jnp.where(alone, c_imag, c_imag - s_real)
                lines[high, :rows] = jnp.where(alone, s_real, c_real - s_imag)
                lines[high, rows:] = jnp.where(alone, s_imag, c_imag + s_real)
        whole = dot_nt(second[...], lines[...].astype(BF16))
        send_two[c] = whole.reshape(peers, step, span).astype(BF16)

    lane_block = lax.broadcasted_iota(jnp.int32, (step, LANES), 1) // narrow

    def arrange(c):
        for d0 in range(0, peers, group):
            for t0 in range(0, peers, group):
                held = [
                    got_two[c, d0 + i, :, t0 * narrow : (t0 + group) * narrow].astype(F32)
                    for i in range(group)
                ]
                stride = group // 2
                while stride:
                    upper = (lane_block // stride) % 2 == 1
                    for i in range(group):
                        if i // stride % 2 == 0:
                            a, b = held[i], held[i + stride]
                            held[i] = jnp.where(upper, pltpu.roll(b, stride * narrow, 1), a)
                            held[i + stride] = jnp.where(
                                upper, b, pltpu.roll(a, LANES - stride * narrow, 1)
                            )
                    stride //= 2
                for j in range(group):
                    arranged[d0 // group, pl.ds(t0 + j, step, stride=peers), :] = held[j]
        for b in range(0, span, LANES):
            at = c * span + b
            mixed_ref[:, at : at + LANES] = arranged[b // LANES].astype(BF16)

    def weigh():
        for c in range(chunks):
            for i in range(cols):
                for b in range(0, block, LANES):
                    high = min(LANES, block)
                    w = w_out[i, :, :, :, c * block + b : c * block + b + high, :]
                    w = w.reshape(peers, high, w.shape[-1])
                    w = jnp.concatenate([w[p] for p in range(peers)], axis=1)
                    at = c * span + i * block + b
                    weight_ref[at : at + high, :] = dot(place_of[:high, :high], w).astype(BF16)

    for c in range(chunks):
        if c:
            push(gather_in[c])
        for part in gather_in[c]:
            part.finish()
        project(c)
        exchange(0, c, send_one.at[c], got_one.at[c])
        if c == 0:
            push(gather_out)

    push(gather_out[: len(gather_out) // 2])
    for c in range(chunks):
        land(0, c)
        transform(c)
        exchange(1, c, send_two.at[c], got_two.at[c])
        if c == 0:
            push(gather_out[len(gather_out) // 2 :])
    push(gather_out)
    last = flights[1, chunks - 1]
    for c in range(chunks):
        land(1, c) if c + 1 < chunks else None
        if c + 1 < chunks:
            arrange(c)
    for part in gather_out:
        part.finish()
    weigh()
    late = {id(copy) for copy in last}
    for copy in sent:
        if id(copy) not in late:
            copy.wait_send()
    land(1, chunks - 1)
    arrange(chunks - 1)
    for copy in last:
        copy.wait_send()


def close(mixed_ref, weight_ref, result_ref, result, store_sem):
    width = result.shape[1]
    piece = min(256, width)
    stores = []
    for i in range(width // piece):
        at = slice(i * piece, (i + 1) * piece)
        result[:, at] = dot(mixed_ref[...], weight_ref[:, at]).astype(BF16)
        store = pltpu.make_async_copy(result.at[:, at], result_ref.at[:, at], store_sem.at[i])
        store.start()
        stores.append(store)
    for store in stores:
        store.wait()


def body(peers, cols, tokens, norm_gain, in_weight, out_weight):
    rows, width = tokens.shape[1:]
    in_rows, in_cols = in_weight.shape
    out_rows, out_cols = out_weight.shape
    channels = in_cols * cols
    depth, tall, wide = grid_of(peers)
    chunks = 2 if in_cols % (2 * LANES) == 0 else 1
    block = in_cols // chunks
    span = block * cols
    narrow = span // peers
    step = rows // peers
    in_parts = max(1, min(4, in_rows // 16))
    out_parts = max(1, min(4, out_rows // 16))
    forward, place_of, first, turn, second = tables(peers, rows, narrow)
    vmem = pl.BlockSpec(memory_space=pltpu.VMEM)
    hbm = pl.BlockSpec(memory_space=pltpu.HBM)
    count = sem_count(peers, cols, chunks * in_parts + out_parts)
    mixed, weight = pl.pallas_call(
        functools.partial(kernel, peers, cols, chunks, in_parts, out_parts),
        out_shape=(
            pltpu.VMEM((rows, channels), BF16),
            pltpu.VMEM((channels, width), BF16),
        ),
        in_specs=[hbm] * 9,
        out_specs=(vmem, vmem),
        scratch_shapes=[
            pltpu.VMEM((rows, width), BF16),
            pltpu.VMEM((width,), BF16),
            pltpu.VMEM(forward.shape, BF16),
            pltpu.VMEM(place_of.shape, BF16),
            pltpu.VMEM(first.shape, BF16),
            pltpu.VMEM(turn.shape, F32),
            pltpu.VMEM(second.shape, BF16),
            pltpu.VMEM((rows, width), BF16),
            pltpu.VMEM((chunks, cols, depth, tall, wide, in_rows, block), BF16),
            pltpu.VMEM((cols, depth, tall, wide, out_rows, out_cols), BF16),
            pltpu.VMEM((chunks, peers, narrow, rows), BF16),
            pltpu.VMEM((chunks, peers, narrow, rows), BF16),
            pltpu.VMEM((span, 2 * rows), F32),
            pltpu.VMEM((chunks, peers, step, span), BF16),
            pltpu.VMEM((chunks, peers, step, span), BF16),
            pltpu.VMEM((span // LANES, rows, LANES), F32),
            pltpu.SemaphoreType.DMA((7,)),
            pltpu.SemaphoreType.DMA((chunks + 2,)),
            pltpu.SemaphoreType.DMA((count,)),
            pltpu.SemaphoreType.DMA((count,)),
        ],
        compiler_params=pltpu.CompilerParams(
            collective_id=0, has_side_effects=True, vmem_limit_bytes=32 * 1024 * 1024
        ),
    )(
        *(
            pltpu.with_memory_space_constraint(a, pltpu.HBM)
            for a in (
                tokens[0],
                norm_gain,
                in_weight,
                out_weight,
                forward,
                place_of,
                first,
                turn,
                second,
            )
        )
    )
    pieces = width // min(256, width)
    result = pl.pallas_call(
        close,
        out_shape=jax.ShapeDtypeStruct((rows, width), BF16),
        in_specs=[vmem, vmem],
        out_specs=hbm,
        scratch_shapes=[
            pltpu.VMEM((rows, width), BF16),
            pltpu.SemaphoreType.DMA((pieces,)),
        ],
        compiler_params=pltpu.CompilerParams(vmem_limit_bytes=16 * 1024 * 1024),
    )(mixed, weight)
    return result[None]


def solution(mesh):
    in_specs = (P("col", "row", None), P(), P("row", "col"), P("col", "row"))
    out_specs = P("col", "row", None)
    step = functools.partial(body, mesh.shape["row"], mesh.shape["col"])
    return jax.shard_map(step, mesh=mesh, in_specs=in_specs, out_specs=out_specs, check_vma=False)
```

time: 55.6 us -> 44.6 us (0.80)
  Pallas kernels: 52.6 us -> 44.1 us
  local copies, waits for them, and re-layouts: 2.73 us -> 0 us
    pallas_call x1 -> x2, Pallas kernels: 52.6 us -> 44.1 us  [the longest x1 42.2 us: body(): pl.pallas_call(functools.partial(kernel, peers, cols, chunks, in_parts, o...]
    unnamed x1 -> x0, local copies, waits for them, and re-layouts: 2.73 us -> none
where the time goes in v1:
time: 44.6 us; the launch traced here: 44.2 us
  Pallas kernels  44.1 us (99%)
    pallas_call x1, Pallas kernels, body(): pl.pallas_call(functools.partial(kernel, peers, cols, chunks, in_parts, o...  42.2 us
    pallas_call x1, Pallas kernels, body(): pl.pallas_call(close, out_shape=jax.ShapeDtypeStruct((rows, width), BF16)...  1.91 us

profile of v1, /device:TPU:0, one launch (start us, length us, event | category | flops | bytes accessed | tf_op | source)
XLA Modules:
  0.0 44.2 jit_solution(8057571221832419196)
XLA Ops:
  0.0 42.2 %shard_map.91 = (bf16[384,512]{1,0:T(8,128)(2,1)S(1)}, bf16[512,2048]{1,0:T(8,128)(2,1)S(1)}) custom-call(bf16[384,2048]{1,0:T(8,128)(2,1)} %bitcast.2, bf16[2048]{0:T(1024)(128)(2,1)} %gain_hbm.1, bf16[128,256]{1,0:T(8,128)(2,1)} %in_hbm.1, bf16[256,128]{1,0:T(8,128)(2,1)} %out_w_hbm.1, bf16[128,128]{1,0:T(8,128)(2,1)} %constant.10.clone.forward_hbm, ...), custom_call_target="tpu_custom_call" | custom-call | tf_op jit(solution)/shard_map/pallas_call | solution.py:453
  42.2 1.9 %shard_map.92 = bf16[384,2048]{1,0:T(8,128)(2,1)} custom-call(bf16[384,512]{1,0:T(8,128)(2,1)S(1)} %get-tuple-element.7.mixed_ref, bf16[512,2048]{1,0:T(8,128)(2,1)S(1)} %get-tuple-element.8.weight_ref), custom_call_target="tpu_custom_call" | custom-call | tf_op jit(solution)/shard_map/pallas_call | solution.py:503

commit v2 on v1

--- a/solution.py
+++ b/solution.py
@@ -83,23 +83,6 @@
 
 def far_first(depth):
     return sorted(range(depth), key=lambda o: abs(2 * o - depth))
-
-
-class Sems:
-    def __init__(self, send, recv):
-        self.send, self.recv, self.used = send, recv, 0
-
-    def next(self):
-        i = self.used
-        self.used += 1
-        assert i < self.send.shape[0]
-        return self.send.at[i], self.recv.at[i]
-
-
-def sem_count(peers, cols, gathers):
-    depth, b, a = grid_of(peers)
-    each = depth - 1 + (a - 1) + (b - 1) + cols - 1
-    return gathers * each + 4 * (peers - 1)
 
 
 def kernel(
@@ -137,8 +120,10 @@
     arranged,
     load_sem,
     own_sem,
-    send_sem,
-    recv_sem,
+    flow_send,
+    flow_recv,
+    swap_send,
+    swap_recv,
 ):
     me = lax.axis_index("row")
     core = lax.axis_index("col")
@@ -153,7 +138,6 @@
     half = narrow // 2
     step = rows // peers
     group = LANES // narrow
-    sems = Sems(send_sem, recv_sem)
 
     def at_peer(dz, dy, dx):
         tz = lax.rem(z + dz, depth)
@@ -200,62 +184,89 @@
         own.wait()
     pl.semaphore_wait(barrier, len(near) + cols - 1)
 
-    sent = []
-
-    def remote(src, dst, device):
-        send, recv = sems.next()
-        copy = pltpu.make_async_remote_copy(
+    def remote(src, dst, send, recv, device):
+        pltpu.make_async_remote_copy(
             src_ref=src, dst_ref=dst, send_sem=send, recv_sem=recv, device_id=device
-        )
-        copy.start()
-        sent.append(copy)
-        return copy
+        ).start()
+
+    def settle(ref, sem):
+        pltpu.make_async_copy(ref, ref, sem).wait()
 
     class Part:
-        def __init__(self, buffer, index, height):
-            self.buffer, self.at, self.flip = buffer, pl.ds(index * height, height), index % 2
-            self.stage, self.open = 0, []
+        def __init__(self, which, index, buffer, height):
+            self.which, self.index, self.buffer = which, index, buffer
+            self.at, self.flip = pl.ds(index * height, height), index % 2
+            self.stage = 0
+
+        def along_x(self, stage):
+            return (stage == 1) != bool(self.flip)
+
+        def extent(self, stage):
+            if stage in (0, 3):
+                return cols if stage else depth
+            return wide if self.along_x(stage) else tall
+
+        def amount(self, stage, at):
+            held = self.buffer.at[core]
+            if stage == 0:
+                return held.at[pl.ds(0, depth - 1), 0, 0, at]
+            if stage == 3:
+                return self.buffer.at[pl.ds(0, cols - 1), :, :, :, at]
+            if stage == 1:
+                return held.at[:, 0, 0, at]
+            return held.at[:, :, 0, at] if self.along_x(stage) else held.at[:, 0, :, at]
+
+        def land(self):
+            if self.stage and self.extent(self.stage - 1) > 1:
+                settle(
+                    self.amount(self.stage - 1, self.at),
+                    flow_recv.at[self.which, self.stage - 1, self.index],
+                )
 
         def push(self):
-            for copy in self.open:
-                copy.wait_recv()
-            held, everything = self.buffer.at[core], slice(None)
-            if self.stage == 0:
-                targets = [
-                    (held.at[z, y, x, self.at], {"row": at_peer(o, 0, 0)})
-                    for o in far_first(depth)
-                    if o
-                ]
-            elif self.stage == 3:
-                targets = [
-                    (held.at[:, :, :, self.at], {"col": mate(o)}) for o in range(1, cols)
-                ]
+            self.land()
+            held, stage = self.buffer.at[core], self.stage
+            if stage == 0:
+                ref = held.at[z, y, x, self.at]
+                targets = [{"row": at_peer(o, 0, 0)} for o in far_first(depth) if o]
+            elif stage == 3:
+                ref = held.at[:, :, :, self.at]
+                targets = [{"col": mate(o)} for o in range(1, cols)]
             else:
-                along_x = (self.stage == 1) != bool(self.flip)
-                if self.stage == 1:
+                along_x = self.along_x(stage)
+                if stage == 1:
                     ref = held.at[:, y, x, self.at]
                 elif along_x:
                     ref = held.at[:, :, x, self.at]
                 else:
                     ref = held.at[:, y, :, self.at]
-                extent = wide if along_x else tall
                 targets = [
-                    (ref, {"row": at_peer(0, 0, o) if along_x else at_peer(0, o, 0)})
-                    for o in range(1, extent)
+                    {"row": at_peer(0, 0, o) if along_x else at_peer(0, o, 0)}
+                    for o in range(1, self.extent(stage))
                 ]
-            self.open = [remote(ref, ref, device) for ref, device in targets]
+            for device in targets:
+                send = flow_send.at[self.which, stage, self.index % 2]
+                recv = flow_recv.at[self.which, stage, self.index]
+                remote(ref, ref, send, recv, device)
             self.stage += 1
 
-        def finish(self):
-            for copy in self.open:
-                copy.wait_recv()
-
-    def parts_of(buffer, count):
+    def parts_of(which, buffer, count):
         height = buffer.shape[-2] // count
-        return [Part(buffer, i, height) for i in range(count)]
-
-    gather_in = [parts_of(w_in.at[c], in_parts) for c in range(chunks)]
-    gather_out = parts_of(w_out, out_parts)
+        return [Part(which, i, buffer, height) for i in range(count)]
+
+    gather_in = [parts_of(c, w_in.at[c], in_parts) for c in range(chunks)]
+    gather_out = parts_of(chunks, w_out, out_parts)
+
+    def drain(parts):
+        for stage in range(4):
+            for side in range(min(2, len(parts))):
+                some = parts[side::2]
+                if some[0].extent(stage) > 1:
+                    settle(
+                        some[0].amount(stage, pl.ds(0, some[0].at.size * len(some))),
+                        flow_send.at[some[0].which, stage, side],
+                    )
+
     def push(parts):
         for part in parts:
             part.push()
@@ -290,24 +301,22 @@
     for load in loads[2:]:
         load.wait()
 
-    flights = {}
-
     def exchange(which, c, src, dst):
-        copies = []
         for dz in far_first(depth):
             for dy in reversed(range(tall)):
                 for dx in reversed(range(wide)):
                     if dz or dy or dx:
                         to = at_peer(dz, dy, dx)
-                        copies.append(remote(src.at[to], dst.at[me], {"row": to}))
+                        send, recv = swap_send.at[which, c], swap_recv.at[which, c]
+                        remote(src.at[to], dst.at[me], send, recv, {"row": to})
         own = pltpu.make_async_copy(src.at[me], dst.at[me], own_sem.at[chunks + 1])
         own.start()
         own.wait()
-        flights[which, c] = copies
-
-    def land(which, c):
-        for copy in flights[which, c]:
-            copy.wait_recv()
+
+    others = pl.ds(0, peers - 1)
+
+    def land(dst, which, c):
+        settle(dst.at[c, others], swap_recv.at[which, c])
 
     def project(c):
         weight = jnp.concatenate(
@@ -387,7 +396,7 @@
         if c:
             push(gather_in[c])
         for part in gather_in[c]:
-            part.finish()
+            part.land()
         project(c)
         exchange(0, c, send_one.at[c], got_one.at[c])
         if c == 0:
@@ -395,28 +404,26 @@
 
     push(gather_out[: len(gather_out) // 2])
     for c in range(chunks):
-        land(0, c)
+        land(got_one, 0, c)
         transform(c)
         exchange(1, c, send_two.at[c], got_two.at[c])
         if c == 0:
             push(gather_out[len(gather_out) // 2 :])
     push(gather_out)
-    last = flights[1, chunks - 1]
+    for c in range(chunks - 1):
+        land(got_two, 1, c)
+        arrange(c)
+    for part in gather_out:
+        part.land()
+    weigh()
+    for parts in gather_in + [gather_out]:
+        drain(parts)
     for c in range(chunks):
-        land(1, c) if c + 1 < chunks else None
-        if c + 1 < chunks:
-            arrange(c)
-    for part in gather_out:
-        part.finish()
-    weigh()
-    late = {id(copy) for copy in last}
-    for copy in sent:
-        if id(copy) not in late:
-            copy.wait_send()
-    land(1, chunks - 1)
+        settle(send_one.at[c, others], swap_send.at[0, c])
+    land(got_two, 1, chunks - 1)
     arrange(chunks - 1)
-    for copy in last:
-        copy.wait_send()
+    for c in range(chunks):
+        settle(send_two.at[c, others], swap_send.at[1, c])
 
 
 def close(mixed_ref, weight_ref, result_ref, result, store_sem):
@@ -449,7 +456,6 @@
     forward, place_of, first, turn, second = tables(peers, rows, narrow)
     vmem = pl.BlockSpec(memory_space=pltpu.VMEM)
     hbm = pl.BlockSpec(memory_space=pltpu.HBM)
-    count = sem_count(peers, cols, chunks * in_parts + out_parts)
     mixed, weight = pl.pallas_call(
         functools.partial(kernel, peers, cols, chunks, in_parts, out_parts),
         out_shape=(
@@ -477,8 +483,10 @@
             pltpu.VMEM((span // LANES, rows, LANES), F32),
             pltpu.SemaphoreType.DMA((7,)),
             pltpu.SemaphoreType.DMA((chunks + 2,)),
-            pltpu.SemaphoreType.DMA((count,)),
-            pltpu.SemaphoreType.DMA((count,)),
+            pltpu.SemaphoreType.DMA((chunks + 1, 4, 2)),
+            pltpu.SemaphoreType.DMA((chunks + 1, 4, max(in_parts, out_parts))),
+            pltpu.SemaphoreType.DMA((2, chunks)),
+            pltpu.SemaphoreType.DMA((2, chunks)),
         ],
         compiler_params=pltpu.CompilerParams(
             collective_id=0, has_side_effects=True, vmem_limit_bytes=32 * 1024 * 1024

time: 44.6 us -> 42.8 us (0.960)
  Pallas kernels: 44.1 us -> 42.4 us
    pallas_call x1, Pallas kernels: 42.2 us -> 40.5 us  [body(): pl.pallas_call(functools.partial(kernel, peers, cols, chunks, in_parts, o...]
where the time goes in v2:
time: 42.8 us; the launch traced here: 42.4 us
  Pallas kernels  42.4 us (99%)
    pallas_call x1, Pallas kernels, body(): pl.pallas_call(functools.partial(kernel, peers, cols, chunks, in_parts, o...  40.5 us
    pallas_call x1, Pallas kernels, body(): pl.pallas_call(close, out_shape=jax.ShapeDtypeStruct((rows, width), BF16)...  1.91 us

profile of v2, /device:TPU:0, one launch (start us, length us, event | category | flops | bytes accessed | tf_op | source)
XLA Modules:
  0.0 42.4 jit_solution(3020997700803474781)
XLA Ops:
  0.0 40.5 %shard_map.91 = (bf16[384,512]{1,0:T(8,128)(2,1)S(1)}, bf16[512,2048]{1,0:T(8,128)(2,1)S(1)}) custom-call(bf16[384,2048]{1,0:T(8,128)(2,1)} %bitcast.2, bf16[2048]{0:T(1024)(128)(2,1)} %gain_hbm.1, bf16[128,256]{1,0:T(8,128)(2,1)} %in_hbm.1, bf16[256,128]{1,0:T(8,128)(2,1)} %out_w_hbm.1, bf16[128,128]{1,0:T(8,128)(2,1)} %constant.10.clone.forward_hbm, ...), custom_call_target="tpu_custom_call" | custom-call | tf_op jit(solution)/shard_map/pallas_call | solution.py:459
  40.5 1.9 %shard_map.92 = bf16[384,2048]{1,0:T(8,128)(2,1)} custom-call(bf16[384,512]{1,0:T(8,128)(2,1)S(1)} %get-tuple-element.7.mixed_ref, bf16[512,2048]{1,0:T(8,128)(2,1)S(1)} %get-tuple-element.8.weight_ref), custom_call_target="tpu_custom_call" | custom-call | tf_op jit(solution)/shard_map/pallas_call | solution.py:511
